TPU v7x, 32 devices: a whole 2x2x4 slice. The times are simulated.
32 devices in a mesh: kv: 8 (over z, y), tp: 4 (over x, core).
Axes of the slice: x: 2, y: 2, z: 4, core: 2. Of those that a mesh axis runs over, the one named last changes fastest.
Arguments:
- tokens: bfloat16 [128, 4096], P(None, ('kv', 'tp')), may hold values from -64 to 64
- mix_gain: float32 [4096], P('kv'), may hold values from 0.1 to 1.9
- w_query: bfloat16 [4096, 3072], P('kv', 'tp'), may hold values from -0.09375 to 0.09375
- w_key: bfloat16 [4096, 3072], P('kv', 'tp'), may hold values from -0.09375 to 0.09375
- w_value: bfloat16 [4096, 3072], P('kv', 'tp'), may hold values from -0.09375 to 0.09375
- w_gate: bfloat16 [4096, 3072], P('kv', 'tp'), may hold values from -0.09375 to 0.09375
- w_beta: bfloat16 [4096, 24], P('kv'), may hold values from -0.09375 to 0.09375
- w_decay: bfloat16 [4096, 24], P('kv'), may hold values from -0.09375 to 0.09375
- decay_rate: float32 [24], P('tp'), may hold values from 0.15 to 1.5
- out_gain: float32 [128], replicated, may hold values from 0.1 to 1.9
- state: float32 [128, 24, 128, 128], P('kv', 'tp'), may hold values from -0.6 to 0.6
- w_out: bfloat16 [3072, 4096], P('tp', 'kv'), may hold values from -0.109375 to 0.109375
- mlp_gain: float32 [4096], replicated, may hold values from 0.1 to 1.9
- w_up: bfloat16 [4096, 16384], P(None, ('kv', 'tp')), may hold values from -0.09375 to 0.09375
- w_down: bfloat16 [16384, 4096], P(('kv', 'tp')), may hold values from -0.09375 to 0.09375
Outputs:
- mixed: bfloat16 [128, 4096], P(None, ('kv', 'tp'))
- new_state: float32 [128, 24, 128, 128], P('kv', 'tp')
All inputs are finite; a program needn't handle non-finite values.
Results may differ from a plain program's by a relative error of at most 0.0063.
Values may be sent and summed in bfloat16 or wider, within the bound.
A program may use at most 64 MiB of HBM per device.

v0:
```python
import jax
import jax.numpy as jnp
from jax import lax
from jax.sharding import PartitionSpec as P

D = 4096


EPSILON = 1e-06


def head_norm(values):
    return values * lax.rsqrt(jnp.sum(values * values, axis=-1, keepdims=True) + EPSILON)


def feed_forward(segment, mlp_gain, w_up, w_down):
    segment_f = segment.astype(jnp.float32)
    normed_mlp = (
        segment_f
        * lax.rsqrt(jnp.mean(segment_f * segment_f, axis=1, keepdims=True) + EPSILON)
        * mlp_gain[None, :]
    ).astype(jnp.bfloat16)
    hidden = jnp.square(
        jax.nn.relu(jnp.dot(normed_mlp, w_up, preferred_element_type=jnp.float32))
    ).astype(jnp.bfloat16)
    return jnp.dot(hidden, w_down, preferred_element_type=jnp.float32)


def local(
    tokens,
    mix_gain,
    w_query,
    w_key,
    w_value,
    w_gate,
    w_beta,
    w_decay,
    decay_rate,
    out_gain,
    state,
    w_out,
    mlp_gain,
    w_up,
    w_down,
):
    local_rows = state.shape[0]
    local_heads = decay_rate.shape[0]
    head_size = state.shape[2]
    all_heads = w_beta.shape[1]
    columns = lax.all_gather(tokens, "tp", axis=1, tiled=True)
    columns_f = columns.astype(jnp.float32)
    normed = (columns_f * mix_gain[None, :]).astype(jnp.bfloat16)
    part_query = jnp.dot(normed, w_query, preferred_element_type=jnp.float32)
    part_key = jnp.dot(normed, w_key, preferred_element_type=jnp.float32)
    part_value = jnp.dot(normed, w_value, preferred_element_type=jnp.float32)
    part_gate = jnp.dot(normed, w_gate, preferred_element_type=jnp.float32)
    part_rates = jnp.dot(
        normed, jnp.concatenate([w_beta, w_decay], axis=1), preferred_element_type=jnp.float32
    )
    summed = (
        lax.psum_scatter(part_query, "kv", scatter_dimension=0, tiled=True),
        lax.psum_scatter(part_key, "kv", scatter_dimension=0, tiled=True),
        lax.psum_scatter(part_value, "kv", scatter_dimension=0, tiled=True),
        lax.psum_scatter(part_gate, "kv", scatter_dimension=0, tiled=True),
        lax.psum_scatter(part_rates, "kv", scatter_dimension=0, tiled=True),
        lax.psum_scatter(
            jnp.sum(columns_f * columns_f, axis=1), "kv", scatter_dimension=0, tiled=True
        ),
    )
    own_squares = summed[5]
    row_scale = lax.rsqrt(own_squares / D + EPSILON)[:, None]
    shape_heads = (local_rows, local_heads, head_size)
    query = head_norm(jax.nn.silu((summed[0] * row_scale).reshape(shape_heads))) * head_size ** (
        -0.5
    )
    key = head_norm(jax.nn.silu((summed[1] * row_scale).reshape(shape_heads)))
    value = jax.nn.silu((summed[2] * row_scale).reshape(shape_heads))
    gate_raw = (summed[3] * row_scale).reshape(shape_heads)
    rates = summed[4] * row_scale
    head_start = lax.axis_index("tp") * local_heads
    beta = jax.nn.sigmoid(lax.dynamic_slice_in_dim(rates, head_start, local_heads, 1))
    decay_raw = lax.dynamic_slice_in_dim(rates, all_heads + head_start, local_heads, 1)
    decay = jnp.exp(-decay_rate[None, :] * jax.nn.softplus(decay_raw))
    faded = state * decay[:, :, None, None]
    recalled = jnp.einsum("bhkv,bhk->bhv", faded, key, precision=lax.Precision.HIGHEST)
    change = beta[:, :, None] * (value - recalled)
    new_state = faded + key[:, :, :, None] * change[:, :, None, :]
    readout = jnp.einsum("bhkv,bhk->bhv", new_state, query, precision=lax.Precision.HIGHEST)
    scaled = (
        readout
        * lax.rsqrt(jnp.mean(readout * readout, axis=-1, keepdims=True) + EPSILON)
        * out_gain
    )
    merged = (
        (scaled * jax.nn.silu(gate_raw))
        .reshape(local_rows, local_heads * head_size)
        .astype(jnp.bfloat16)
    )
    partial_out = jnp.dot(
        lax.all_gather(merged, "kv", axis=0, tiled=True), w_out, preferred_element_type=jnp.float32
    )
    branch_sum = lax.psum_scatter(partial_out, "tp", scatter_dimension=1, tiled=True)
    residual = (tokens.astype(jnp.float32) + branch_sum).astype(jnp.bfloat16)
    whole_rows = lax.all_gather(residual, ("kv", "tp"), axis=1, tiled=True)
    partial_mlp = feed_forward(whole_rows, mlp_gain, w_up, w_down)
    branch = lax.psum_scatter(partial_mlp, ("kv", "tp"), scatter_dimension=1, tiled=True)
    mixed = (residual.astype(jnp.float32) + branch).astype(jnp.bfloat16)
    return (mixed, new_state)


def solution(mesh):
    placed = (
        P(None, ("kv", "tp")),
        P("kv"),
        P("kv", "tp"),
        P("kv", "tp"),
        P("kv", "tp"),
        P("kv", "tp"),
        P("kv", None),
        P("kv", None),
        P("tp"),
        P(),
        P("kv", "tp", None, None),
        P("tp", "kv"),
        P(),
        P(None, ("kv", "tp")),
        P(("kv", "tp"), None),
    )
    return jax.shard_map(
        local,
        mesh=mesh,
        in_specs=placed,
        out_specs=(P(None, ("kv", "tp")), P("kv", "tp", None, None)),
        check_vma=False,
    )
```

profile of v0, /device:TPU:0, one launch (start us, length us, event | category | flops | bytes accessed | tf_op | source)
XLA Modules:
  0.0 618.0 jit_solution(8560261450145057802)
XLA Ops:
  7.2 0.0 copy-start
  7.2 0.0 copy-start.11
  7.2 0.0 copy-start.7
  7.2 0.0 copy-start.2
  7.2 0.0 copy-start.3
  7.2 0.0 copy-start.10
  7.2 0.0 reduce-scatter.8.cloned.1.call-start
  7.3 6.9 %all_gather.9 = bf16[128,512]{1,0:T(8,128)(2,1)S(1)} all-gather(bf16[128,128]{1,0:T(8,128)(2,1)} %param.15), channel_id=1, replica_groups=mesh['kv'=8,'tp'=4] {'tp'}, dimensions={1}, use_global_device_ids=true | all-gather | bytes 163840 | tf_op jit(solution)/shard_map/all_gather | solution.py:50
  14.2 1.6 fusion.31
  15.7 0.0 reduce-scatter.8.cloned.1.call-update
  15.8 0.0 reduce-scatter.10.cloned.1.call-start
  15.8 1.7 fusion.29
  17.5 0.0 reduce-scatter.10.cloned.1.call-update
  17.5 0.0 reduce-scatter.12.cloned.1.call-start
  17.6 2.2 fusion.27
  19.8 0.0 reduce-scatter.12.cloned.1.call-update
  19.8 0.0 reduce-scatter.14.cloned.1.call-start
  19.8 1.7 fusion.25
  21.5 0.0 reduce-scatter.14.cloned.1.call-update
  21.6 0.0 reduce-scatter.16.cloned.1.call-start
  21.6 1.0 fusion.23
  22.7 0.0 reduce-scatter.16.cloned.1.call-update
  22.7 0.0 reduce-scatter.18.cloned.1.call-start
  22.8 0.6 dynamic-slice
  24.0 0.1 fusion.16
  24.1 22.1 %all-reduce = f32[128]{0:T(128)S(1)} all-reduce(f32[128]{0:T(128)S(1)} %fusion.16), channel_id=3, replica_groups=mesh['kv'=8,'tp'=4] {'kv'}, use_global_device_ids=true, to_apply=%region_2.0.clone | all-reduce | flops 128 | bytes 1024
  46.2 0.1 fusion.42
  46.3 33.7 %reduce-scatter.8.cloned.1.call-done = f32[16,48]{1,0:T(8,128)} async-done(((f32[128,48]{1,0:T(8,128)}), f32[16,48]{1,0:T(8,128)}) %reduce-scatter.8.cloned.1.call-update) | async-done | bytes 3088 | tf_op jit(solution)/shard_map/reduce_scatter | solution.py:65
  80.0 0.8 broadcast_multiply_fusion.5
  80.8 0.1 add_divide_fusion
  80.9 63.6 %reduce-scatter.10.cloned.1.call-done = f32[16,768]{1,0:T(8,128)} async-done(((f32[128,768]{1,0:T(8,128)}), f32[16,768]{1,0:T(8,128)}) %reduce-scatter.10.cloned.1.call-update) | async-done | bytes 49168 | tf_op jit(solution)/shard_map/reduce_scatter | solution.py:62
  144.5 64.5 %reduce-scatter.12.cloned.1.call-done = f32[16,768]{1,0:T(8,128)} async-done(((f32[128,768]{1,0:T(8,128)}), f32[16,768]{1,0:T(8,128)}) %reduce-scatter.12.cloned.1.call-update) | async-done | bytes 49168 | tf_op jit(solution)/shard_map/reduce_scatter | solution.py:63
  209.0 64.3 %reduce-scatter.14.cloned.1.call-done = f32[16,768]{1,0:T(8,128)} async-done(((f32[128,768]{1,0:T(8,128)}), f32[16,768]{1,0:T(8,128)}) %reduce-scatter.14.cloned.1.call-update) | async-done | bytes 49168 | tf_op jit(solution)/shard_map/reduce_scatter | solution.py:61
  273.3 64.9 %reduce-scatter.16.cloned.1.call-done = f32[16,768]{1,0:T(8,128)} async-done(((f32[128,768]{1,0:T(8,128)}), f32[16,768]{1,0:T(8,128)}) %reduce-scatter.16.cloned.1.call-update) | async-done | bytes 49168 | tf_op jit(solution)/shard_map/reduce_scatter | solution.py:64
  338.2 1.0 broadcast_multiply_fusion.1
  339.2 0.1 multiply_reduce_fusion.1
  339.3 0.1 fusion.55
  339.4 0.1 broadcast_multiply_fusion
  339.5 0.1 multiply_reduce_fusion
  339.6 0.1 multiply_bitcast_fusion
  339.7 7.7 %fusion = f32[16,6,1,128]{3,2,1,0:T(1,128)S(1)} fusion(f32[16,6,128,128]{3,2,1,0:T(8,128)} %param.25, f32[16,6]{1,0:T(8,128)S(1)} %get-tuple-element.3, f32[16,6,128,1]{2,1,0,3:T(8,128)S(1)} %fusion.55), kind=kOutput, calls=%fused_computation.1 | convolution fusion | flops 20447232 | bytes 6390144 | tf_op jit(solution)/shard_map/bhkv,bhk->bhv/dot_general | solution.py:85
  347.5 0.1 fusion.22
  347.6 4.5 multiply_add_fusion
  352.1 0.0 copy-start.1
  352.1 2.7 copy-done.1
  354.8 5.4 fusion.36
  360.2 0.1 fusion.18
  360.3 0.1 fusion.21
  360.4 30.7 %all_gather.10 = bf16[128,768]{1,0:T(8,128)(2,1)S(1)} all-gather(bf16[16,768]{1,0:T(8,128)(2,1)S(1)} %bitcast.34), channel_id=1, replica_groups=mesh['kv'=8,'tp'=4] {'kv'}, dimensions={0}, use_global_device_ids=true | all-gather | bytes 221184 | tf_op jit(solution)/shard_map/all_gather | solution.py:100
  391.2 0.0 copy-done.4
  391.2 1.0 fusion.45
  392.1 0.0 reduce-scatter.18.cloned.1.call-update
  392.2 0.0 all-gather.2.cloned.1.call-start
  392.2 19.3 %reduce-scatter.18.cloned.1.call-done = f32[128,128]{1,0:T(8,128)} async-done(((f32[128,512]{1,0:T(8,128)}), f32[128,128]{1,0:T(8,128)}) %reduce-scatter.18.cloned.1.call-update) | async-done | bytes 65552 | tf_op jit(solution)/shard_map/reduce_scatter | solution.py:102
  411.5 1.5 add_convert_fusion.1
  412.9 0.0 all-gather.2.cloned.1.call-update
  413.0 0.0 reduce-scatter.20.cloned.1.call-start
  413.0 50.4 %all-gather.2.cloned.1.call-done = bf16[128,4096]{1,0:T(8,128)(2,1)} async-done(((bf16[128,128]{1,0:T(8,128)(2,1)}), bf16[128,4096]{1,0:T(8,128)(2,1)}) %all-gather.2.cloned.1.call-update) | async-done | bytes 1048592 | tf_op jit(solution)/shard_map/all_gather | solution.py:104
  463.4 1.5 fusion.3
  464.9 0.0 copy-start.5
  464.9 6.6 %fusion.8 = f32[128,4096]{1,0:T(8,128)} fusion(bf16[512,4096]{1,0:T(8,128)(2,1)} %param.29, bf16[4096,512]{1,0:T(8,128)(2,1)} %param.28, bf16[128,4096]{1,0:T(8,128)(2,1)} %all-gather.2.cloned.1.call-done, f32[4096]{0:T(1024)S(1)} %copy-done.8, f32[128]{0:T(128)S(1)} %add_rsqrt_fusion.3), kind=kOutput, calls=%fused_computation.12 | convolution fusion | flops 1076035584 | bytes 11551232 | tf_op jit(solution)/shard_map/dot_general | solution.py:26
  471.5 0.0 reduce-scatter.20.cloned.1.call-update
  471.5 138.2 %reduce-scatter.20.cloned.1.call-done = f32[128,128]{1,0:T(8,128)} async-done(((f32[128,4096]{1,0:T(8,128)}), f32[128,128]{1,0:T(8,128)}) %reduce-scatter.20.cloned.1.call-update) | async-done | bytes 65552 | tf_op jit(solution)/shard_map/reduce_scatter | solution.py:106
  609.7 1.5 add_convert_fusion
  (24 shorter events, 0.1 us)
Async XLA Ops:
  7.2 8.6 %copy-start = (bf16[512,768]{1,0:T(8,128)(2,1)S(1)}, bf16[512,768]{1,0:T(8,128)(2,1)}, u32[]{:S(2)}) copy-start(bf16[512,768]{1,0:T(8,128)(2,1)} %param.18) | copy-start | bytes 2359300
  7.2 15.6 %copy-start.11 = (u32[32]{0:T(128)S(1)}, u32[32]{0:T(128)}, u32[]{:S(2)}) copy-start(u32[32]{0:T(128)} %constant.45) | copy-start | bytes 388
  7.2 14.4 %copy-start.7 = (f32[512]{0:T(512)S(1)}, f32[512]{0:T(512)}, u32[]{:S(2)}) copy-start(f32[512]{0:T(512)} %param.16) | copy-start | bytes 6148
  7.2 12.6 %copy-start.2 = (bf16[512,768]{1,0:T(8,128)(2,1)S(1)}, bf16[512,768]{1,0:T(8,128)(2,1)}, u32[]{:S(2)}) copy-start(bf16[512,768]{1,0:T(8,128)(2,1)} %param.17) | copy-start | bytes 2359300
  7.2 14.4 %copy-start.3 = (bf16[512,768]{1,0:T(8,128)(2,1)S(1)}, bf16[512,768]{1,0:T(8,128)(2,1)}, u32[]{:S(2)}) copy-start(bf16[512,768]{1,0:T(8,128)(2,1)} %param.20) | copy-start | bytes 2359300
  7.2 15.5 %copy-start.10 = (f32[6]{0:T(128)S(1)}, f32[6]{0:T(128)}, u32[]{:S(2)}) copy-start(f32[6]{0:T(128)} %param.23) | copy-start | bytes 76
  7.2 72.8 %reduce-scatter.8.cloned.1.call-start = ((), (), s32[]{:S(2)}) async-start(), calls=%async_computation.7 | async-start | bytes 73728 | tf_op jit(solution)/shard_map/reduce_scatter | solution.py:65
  15.8 128.7 %reduce-scatter.10.cloned.1.call-start = ((), (), s32[]{:S(2)}) async-start(), calls=%async_computation.8 | async-start | bytes 442368 | tf_op jit(solution)/shard_map/reduce_scatter | solution.py:62
  17.5 191.4 %reduce-scatter.12.cloned.1.call-start = ((), (), s32[]{:S(2)}) async-start(), calls=%async_computation.9 | async-start | bytes 442368 | tf_op jit(solution)/shard_map/reduce_scatter | solution.py:63
  19.8 253.5 %reduce-scatter.14.cloned.1.call-start = ((), (), s32[]{:S(2)}) async-start(), calls=%async_computation.10 | async-start | bytes 442368 | tf_op jit(solution)/shard_map/reduce_scatter | solution.py:61
  21.6 316.6 %reduce-scatter.16.cloned.1.call-start = ((), (), s32[]{:S(2)}) async-start(), calls=%async_computation.11 | async-start | bytes 442368 | tf_op jit(solution)/shard_map/reduce_scatter | solution.py:64
  22.7 388.8 %reduce-scatter.18.cloned.1.call-start = ((), (), s32[]{:S(2)}) async-start(), calls=%async_computation.12 | async-start | bytes 327680 | tf_op jit(solution)/shard_map/reduce_scatter | solution.py:102
  352.1 2.7 copy-start.1
  354.8 5.6 copy-start.9
  354.8 36.4 %copy-start.4 = (bf16[768,512]{1,0:T(8,128)(2,1)S(1)}, bf16[768,512]{1,0:T(8,128)(2,1)}, u32[]{:S(2)}) copy-start(bf16[768,512]{1,0:T(8,128)(2,1)} %param.26) | copy-start | bytes 2359300
  354.8 56.7 %copy-start.6 = (bf16[128,128]{1,0:T(8,128)(2,1)S(1)}, bf16[128,128]{1,0:T(8,128)(2,1)}, u32[]{:S(2)}) copy-start(bf16[128,128]{1,0:T(8,128)(2,1)} %param.15) | copy-start | bytes 98308
  354.8 110.1 %copy-start.8 = (f32[4096]{0:T(1024)S(1)}, f32[4096]{0:T(1024)}, u32[]{:S(2)}) copy-start(f32[4096]{0:T(1024)} %param.27) | copy-start | bytes 49156
  392.2 71.2 %all-gather.2.cloned.1.call-start = ((), (), s32[]{:S(2)}) async-start(), calls=%async_computation.13 | async-start | bytes 1081344 | tf_op jit(solution)/shard_map/all_gather | solution.py:104
  413.0 196.7 %reduce-scatter.20.cloned.1.call-start = ((), (), s32[]{:S(2)}) async-start(), calls=%async_computation.14 | async-start | bytes 2162688 | tf_op jit(solution)/shard_map/reduce_scatter | solution.py:106
  464.9 144.8 %copy-start.5 = (bf16[128,128]{1,0:T(8,128)(2,1)S(1)}, bf16[128,128]{1,0:T(8,128)(2,1)}, u32[]{:S(2)}) copy-start(bf16[128,128]{1,0:T(8,128)(2,1)} %add_convert_fusion.1) | copy-start | bytes 98308
Sparse Core Ops, SparseCore 0:
  15.9 64.0 reduce-scatter.7
  83.3 61.1 reduce-scatter.9
  147.8 61.1 reduce-scatter.11
  212.1 61.1 reduce-scatter.13
  277.0 61.1 reduce-scatter.15
  392.3 19.1 reduce-scatter.17
  414.9 48.4 all-gather.1
  471.6 138.0 reduce-scatter.19
where the time goes:
time: 619 us; the launch traced here: 618 us
  waiting for transfers between devices  499 us (81%)
  blocking collectives  59.7 us (10%)
  matrix products  28.8 us (5%)
  between operations  15.1 us (2%)
  other arithmetic  11.7 us (2%)
    reduce_scatter x1, waiting for transfers between devices, local(): lax.psum_scatter(partial_mlp, ('kv', 'tp'), scatter_dimension=1, tiled=True)  138 us
    reduce_scatter x1, waiting for transfers between devices, local(): lax.psum_scatter(part_gate, 'kv', scatter_dimension=0, tiled=True)  64.9 us
    reduce_scatter x1, waiting for transfers between devices, local(): lax.psum_scatter(part_value, 'kv', scatter_dimension=0, tiled=True)  64.5 us
    reduce_scatter x1, waiting for transfers between devices, local(): lax.psum_scatter(part_query, 'kv', scatter_dimension=0, tiled=True)  64.3 us
    reduce_scatter x1, waiting for transfers between devices, local(): lax.psum_scatter(part_key, 'kv', scatter_dimension=0, tiled=True)  63.6 us
    all_gather x1, waiting for transfers between devices, local(): whole_rows = lax.all_gather(residual, ('kv', 'tp'), axis=1, tiled=True)  50.4 us
    reduce_scatter x1, waiting for transfers between devices, local(): lax.psum_scatter(part_rates, 'kv', scatter_dimension=0, tiled=True)  33.7 us
    all_gather x1, blocking collectives, local(): lax.all_gather(merged, 'kv', axis=0, tiled=True)  30.7 us
  transfers between devices with their start and end apart: 8, of which 8 were waited for; matrix products, arithmetic and copies ran while one was open for 1% of the time, Pallas kernels for 0%

commit v1 on v0

v1 whole, which is shorter than its diff:
```python
import functools
import math

import jax
import jax.numpy as jnp
from jax import lax
from jax.experimental import pallas as pl
from jax.experimental.pallas import tpu as pltpu
from jax.sharding import PartitionSpec as P

EPSILON = 1e-06
CORES = 2
VMEM_BYTES = 60 * 2**20
BF16 = jnp.bfloat16
F32 = jnp.float32


class Grid:
    def __init__(self, n_kv, n_tp):
        self.n_kv, self.n_tp = n_kv, n_tp
        low = max(f for f in range(1, math.isqrt(n_kv) + 1) if n_kv % f == 0)
        self.n_lo, self.n_hi = low, n_kv // low
        self.n_core = CORES if n_tp % CORES == 0 else 1
        self.n_x = n_tp // self.n_core
        self.plane = [
            (dy, dx) for dy in range(self.n_lo) for dx in range(self.n_x) if (dy, dx) != (0, 0)
        ]

    def locate(self):
        self.kv, self.tp = lax.axis_index("kv"), lax.axis_index("tp")
        self.hi, self.lo = self.kv // self.n_lo, lax.rem(self.kv, self.n_lo)
        self.x, self.core = self.tp // self.n_core, lax.rem(self.tp, self.n_core)

    def at(self, hi, lo, x, core):
        return (hi * self.n_lo + lo, x * self.n_core + core)


def step(index, offset, size):
    return lax.rem(index + (offset % size), size) if offset % size else index


def send(src, dst, send_sem, recv_sem, device):
    copy = pltpu.make_async_remote_copy(
        src_ref=src,
        dst_ref=dst,
        send_sem=send_sem,
        recv_sem=recv_sem,
        device_id=device,
        device_id_type=pl.DeviceIdType.MESH,
    )
    copy.start()
    return copy


def greet(peers):
    barrier = pltpu.get_barrier_semaphore()
    for peer in peers:
        pl.semaphore_signal(barrier, inc=1, device_id=peer, device_id_type=pl.DeviceIdType.MESH)
    pl.semaphore_wait(barrier, len(peers))


def project_kernel(
    grid, rate_width,
    tok_ref, gain_ref, wq_ref, wk_ref, wv_ref, wg_ref, wr_ref,
    out_ref, rate_ref,
    cols, part, rate_part, near_send, near_recv, far_send, far_recv, rate_recv,
    own_sem, tok_sems, near_sems, far_sems, rate_sems,
):
    g = grid
    g.locate()
    n_kv, n_tp, n_lo, n_hi = g.n_kv, g.n_tp, g.n_lo, g.n_hi
    local = pltpu.make_async_copy(tok_ref, cols.at[g.tp], own_sem)
    local.start()
    greet(
        [(g.kv, step(g.tp, k, n_tp)) for k in range(1, n_tp)]
        + [(step(g.kv, k, n_kv), g.tp) for k in range(1, n_kv)]
    )
    started = [
        send(tok_ref, cols.at[g.tp], tok_sems.at[0, k], tok_sems.at[1, k],
             (g.kv, step(g.tp, k, n_tp)))
        for k in range(1, n_tp)
    ]
    local.wait()
    for copy in started:
        copy.wait()
    size = tok_ref.shape[1]
    rows = part.shape[2]
    blocks = [cols[i].astype(F32) for i in range(n_tp)]
    squares = sum(jnp.sum(b * b, axis=1, keepdims=True) for b in blocks)
    normed = [(blocks[i] * gain_ref[i]).astype(BF16) for i in range(n_tp)]
    if size % 128 == 0:
        normed = [jnp.concatenate(normed, axis=1)]
    depth = normed[0].shape[1]

    def product(w_ref):
        return sum(
            jnp.dot(normed[i], w_ref[i * depth : (i + 1) * depth, :], preferred_element_type=F32)
            for i in range(len(normed))
        )

    rates = product(wr_ref)
    lane = lax.broadcasted_iota(jnp.int32, rates.shape, 1)
    rates = jnp.where(lane == rate_width, squares, rates)
    rate_part[...] = rates.reshape(n_kv, rows, rates.shape[1])
    rate_copies = [
        send(rate_part.at[step(g.kv, k, n_kv)], rate_recv.at[k], rate_sems.at[0, k],
             rate_sems.at[1, k], (step(g.kv, k, n_kv), g.tp))
        for k in range(1, n_kv)
    ]
    near = {}
    for c, w_ref in enumerate((wq_ref, wk_ref, wv_ref, wg_ref)):
        value = product(w_ref).reshape(n_kv, rows, w_ref.shape[1])
        part[c] = value
        for lo in range(n_lo):
            for hi in range(n_hi):
                near_send[c, lo, hi] = value[hi * n_lo + lo].astype(BF16)
        for k in range(1, n_lo):
            lo = step(g.lo, k, n_lo)
            near[c, k] = send(near_send.at[c, lo], near_recv.at[c, k], near_sems.at[0, c, k],
                              near_sems.at[1, c, k], (g.hi * n_lo + lo, g.tp))
    far = {}
    for c in range(4):
        for k in range(1, n_lo):
            near[c, k].wait()
        for d in list(range(1, n_hi)) + [0]:
            hi = step(g.hi, d, n_hi)
            total = part[c, hi * n_lo + g.lo]
            for k in range(1, n_lo):
                total = total + near_recv[c, k, hi].astype(F32)
            if d == 0:
                out_ref[c] = total
            else:
                far_send[c, d] = total.astype(BF16)
                far[c, d] = send(far_send.at[c, d], far_recv.at[c, d], far_sems.at[0, c, d],
                                 far_sems.at[1, c, d], (hi * n_lo + g.lo, g.tp))
    for copy in rate_copies:
        copy.wait()
    rate_total = rate_part[g.kv]
    for k in range(1, n_kv):
        rate_total = rate_total + rate_recv[k]
    rate_ref[...] = rate_total
    for c in range(4):
        total = out_ref[c]
        for d in range(1, n_hi):
            far[c, d].wait()
            total = total + far_recv[c, d].astype(F32)
        out_ref[c] = total


def project(grid, tokens, mix_gain, weights, w_rates, rate_width):
    g = grid
    batch, size = tokens.shape
    rows, width = batch // g.n_kv, weights[0].shape[1]
    lanes = w_rates.shape[1]
    vmem = pl.BlockSpec(memory_space=pltpu.VMEM)
    dma = pltpu.SemaphoreType.DMA
    return pl.pallas_call(
        functools.partial(project_kernel, g, rate_width),
        out_shape=(
            jax.ShapeDtypeStruct((4, rows, width), F32),
            jax.ShapeDtypeStruct((rows, lanes), F32),
        ),
        in_specs=[vmem] * 7,
        out_specs=(vmem, vmem),
        scratch_shapes=[
            pltpu.VMEM((g.n_tp, batch, size), BF16),
            pltpu.VMEM((4, g.n_kv, rows, width), F32),
            pltpu.VMEM((g.n_kv, rows, lanes), F32),
            pltpu.VMEM((4, g.n_lo, g.n_hi, rows, width), BF16),
            pltpu.VMEM((4, g.n_lo, g.n_hi, rows, width), BF16),
            pltpu.VMEM((4, g.n_hi, rows, width), BF16),
            pltpu.VMEM((4, g.n_hi, rows, width), BF16),
            pltpu.VMEM((g.n_kv, rows, lanes), F32),
            dma,
            dma((2, g.n_tp)),
            dma((2, 4, g.n_lo)),
            dma((2, 4, g.n_hi)),
            dma((2, g.n_kv)),
        ],
        compiler_params=pltpu.CompilerParams(
            collective_id=0, has_side_effects=True, vmem_limit_bytes=VMEM_BYTES
        ),
        name="project",
    )(tokens, mix_gain.reshape(g.n_tp, 1, size), *weights, w_rates)


def state_kernel(s_ref, kt_ref, qt_ref, value_ref, gate_ref, decay_ref, beta_ref, gain_ref,
                 new_ref, merged_ref):
    for h in range(s_ref.shape[1]):
        row = slice(h, h + 1)
        faded = s_ref[0, h] * decay_ref[0, row, :]
        key = kt_ref[0, :, row]
        recalled = jnp.sum(faded * key, axis=0, keepdims=True)
        change = beta_ref[0, row, :] * (value_ref[0, row, :] - recalled)
        updated = faded + key * change
        new_ref[0, h] = updated
        readout = jnp.sum(updated * qt_ref[0, :, row], axis=0, keepdims=True)
        scaled = (
            readout
            * lax.rsqrt(jnp.mean(readout * readout, axis=1, keepdims=True) + EPSILON)
            * gain_ref[...]
        )
        merged_ref[0, row, :] = scaled * gate_ref[0, row, :]


def update_state(state, key, query, value, gate, decay, beta, out_gain):
    rows, heads, size, _ = state.shape
    whole = pl.BlockSpec((1, heads, size, size), lambda i: (i, 0, 0, 0))
    tall = pl.BlockSpec((1, size, heads), lambda i: (i, 0, 0))
    wide = pl.BlockSpec((1, heads, size), lambda i: (i, 0, 0))
    return pl.pallas_call(
        state_kernel,
        grid=(rows,),
        out_shape=(
            jax.ShapeDtypeStruct(state.shape, F32),
            jax.ShapeDtypeStruct((rows, heads, size), F32),
        ),
        in_specs=[whole, tall, tall, wide, wide, wide, wide,
                  pl.BlockSpec((1, size), lambda i: (0, 0))],
        out_specs=(whole, wide),
        compiler_params=pltpu.CompilerParams(dimension_semantics=("arbitrary",)),
        name="state",
    )(
        state,
        jnp.swapaxes(key, 1, 2),
        jnp.swapaxes(query, 1, 2),
        value,
        gate,
        jnp.broadcast_to(decay[:, :, None], value.shape),
        jnp.broadcast_to(beta[:, :, None], value.shape),
        out_gain.reshape(1, size),
    )


def tail_kernel(
    grid,
    merged_ref, tok_ref, gain_ref, wout_hbm, wup_hbm, wdown_hbm,
    out_ref,
    wout, wup, wdown, mg, rs_own, rs_send, rs_recv, gathered, acc,
    y_own, y_send, y_recv, p_send, p_recv, far_total, f_send, f_recv,
    load_sems, own_sem, mg_sems, rs_sems, ghi_sems, gpl_sems, gco_sems, y_sems, p_sems, f_sems,
):
    g = grid
    g.locate()
    n_kv, n_tp, n_lo, n_hi, n_x = g.n_kv, g.n_tp, g.n_lo, g.n_hi, g.n_x
    batch, size = tok_ref.shape
    loads = [
        pltpu.make_async_copy(src, dst, load_sems.at[i])
        for i, (src, dst) in enumerate(((wout_hbm, wout), (wup_hbm, wup), (wdown_hbm, wdown)))
    ]
    for load in loads:
        load.start()
    local = pltpu.make_async_copy(merged_ref, mg.at[g.kv], own_sem)
    local.start()
    kv_peers = [(step(g.kv, k, n_kv), g.tp) for k in range(1, n_kv)]
    tp_peers = [(g.kv, step(g.tp, k, n_tp)) for k in range(1, n_tp)]
    plane_peers = {
        (dy, dx): g.at(g.hi, step(g.lo, dy, n_lo), step(g.x, dx, n_x), g.core)
        for dy, dx in g.plane
    }
    greet(kv_peers + tp_peers + [plane_peers[d] for d in g.plane if d[0] and d[1]])

    started = [
        send(merged_ref, mg.at[g.kv], mg_sems.at[0, k], mg_sems.at[1, k], kv_peers[k - 1])
        for k in range(1, n_kv)
    ]
    loads[0].wait()
    local.wait()
    for copy in started:
        copy.wait()
    rows = mg.shape[1]
    partial = jnp.dot(
        mg[...].reshape(n_kv * rows, mg.shape[2]), wout[...], preferred_element_type=F32
    )
    for t in range(n_tp):
        block = partial[:, t * size : (t + 1) * size]
        rs_own[t] = block
        rs_send[t] = block.astype(BF16)
    started = [
        send(rs_send.at[step(g.tp, k, n_tp)], rs_recv.at[k], rs_sems.at[0, k], rs_sems.at[1, k],
             tp_peers[k - 1])
        for k in range(1, n_tp)
    ]
    branch = rs_own[g.tp]
    for k in range(1, n_tp):
        started[k - 1].wait()
        branch = branch + rs_recv[k].astype(F32)
    residual = (tok_ref[...].astype(F32) + branch).astype(BF16)

    def index(dz, dy, dx, core):
        kv, tp = g.at(step(g.hi, -dz, n_hi), step(g.lo, -dy, n_lo), step(g.x, -dx, n_x), core)
        return kv * n_tp + tp

    mine = index(0, 0, 0, g.core)
    gathered[mine] = residual
    pending = []
    sibling = None if g.n_core == 1 else g.at(g.hi, g.lo, g.x, 1 - g.core)

    def to_sibling(dz, dy, dx):
        if sibling is None:
            return
        place = gathered.at[index(dz, dy, dx, g.core)]
        slot = (dz * n_lo + dy) * n_x + dx
        send(place, place, gco_sems.at[0, slot], gco_sems.at[1, slot], sibling)
        other = gathered.at[index(dz, dy, dx, 1 - g.core)]
        pending.append((place, other, gco_sems.at[0, slot], gco_sems.at[1, slot]))

    def wait_for(src, dst, send_sem, recv_sem, device):
        copy = pltpu.make_async_remote_copy(
            src_ref=src, dst_ref=dst, send_sem=send_sem, recv_sem=recv_sem,
            device_id=device, device_id_type=pl.DeviceIdType.MESH,
        )
        copy.wait_recv()

    sent = []
    own = gathered.at[mine]
    for dz in range(1, n_hi):
        peer = g.at(step(g.hi, dz, n_hi), g.lo, g.x, g.core)
        sent.append(send(own, own, ghi_sems.at[0, dz], ghi_sems.at[1, dz], peer))
    for dz in range(n_hi):
        place = gathered.at[index(dz, 0, 0, g.core)]
        if dz:
            wait_for(own, place, ghi_sems.at[0, dz], ghi_sems.at[1, dz],
                     g.at(step(g.hi, dz, n_hi), g.lo, g.x, g.core))
        for p, d in enumerate(g.plane):
            sent.append(send(place, place, gpl_sems.at[0, dz, p], gpl_sems.at[1, dz, p],
                             plane_peers[d]))
        to_sibling(dz, 0, 0)
    for dz in range(n_hi):
        for p, (dy, dx) in enumerate(g.plane):
            place = gathered.at[index(dz, dy, dx, g.core)]
            wait_for(own, place, gpl_sems.at[0, dz, p], gpl_sems.at[1, dz, p],
                     plane_peers[dy, dx])
            to_sibling(dz, dy, dx)
    for copy in sent:
        copy.wait_send()
    for place, other, send_sem, recv_sem in pending:
        copy = pltpu.make_async_remote_copy(
            src_ref=place, dst_ref=other, send_sem=send_sem, recv_sem=recv_sem,
            device_id=sibling, device_id_type=pl.DeviceIdType.MESH,
        )
        copy.wait_recv()
        copy.wait_send()

    n_dev = n_kv * n_tp
    features = n_dev * size

    def add_squares(i, total):
        block = gathered[i].astype(F32)
        return total + jnp.sum(block * block, axis=1, keepdims=True)

    squares = lax.fori_loop(0, n_dev, add_squares, jnp.zeros((batch, 1), F32))
    scale = lax.rsqrt(squares / features + EPSILON)
    group = n_tp if size % 128 == 0 else 1
    loads[1].wait()
    acc[...] = jnp.zeros_like(acc)

    @pl.loop(0, n_dev // group)
    def _(i):
        parts = [
            (gathered[i * group + j].astype(F32) * scale * gain_ref[i * group + j]).astype(BF16)
            for j in range(group)
        ]
        block = parts[0] if group == 1 else jnp.concatenate(parts, axis=1)
        depth = group * size
        acc[...] += jnp.dot(
            block, wup[pl.ds(pl.multiple_of(i * depth, depth), depth), :],
            preferred_element_type=F32,
        )

    hidden = jnp.square(jnp.maximum(acc[...], 0.0)).astype(BF16)
    loads[2].wait()
    width = n_tp * size

    def down(j):
        columns = pl.ds(pl.multiple_of(j * width, width), width)
        value = jnp.dot(hidden, wdown[:, columns], preferred_element_type=F32)
        for x in range(n_x):
            pair = [
                value[:, (x * g.n_core + c) * size : (x * g.n_core + c + 1) * size]
                for c in range(g.n_core)
            ]
            if g.n_core == 1:
                y_own[j, x] = pair[0]
            else:
                y_own[j, x] = jnp.where(g.core == 0, pair[0], pair[1])
                y_send[j, x] = jnp.where(g.core == 0, pair[1], pair[0]).astype(BF16)

    order = [(dz, dy) for dz in list(range(1, n_hi)) + [0] for dy in range(n_lo)]

    def kv_of(dz, dy):
        return step(g.hi, dz, n_hi) * n_lo + step(g.lo, dy, n_lo)

    swaps = {}
    for s, (dz, dy) in enumerate(order):
        j = kv_of(dz, dy)
        down(j)
        if sibling is not None:
            swaps[dz, dy] = send(y_send.at[j], y_recv.at[j], y_sems.at[0, s], y_sems.at[1, s],
                                 sibling)
    planes = {}
    for dz, dy in order:
        j = kv_of(dz, dy)
        if sibling is not None:
            swaps[dz, dy].wait()
        for dx in range(n_x):
            x = step(g.x, dx, n_x)
            total = y_own[j, x]
            if sibling is not None:
                total = total + y_recv[j, x].astype(F32)
            if (dy, dx) == (0, 0):
                far_total[dz] = total
            else:
                p = g.plane.index((dy, dx))
                p_send[dz, p] = total.astype(BF16)
                planes[dz, p] = send(p_send.at[dz, p], p_recv.at[dz, p], p_sems.at[0, dz, p],
                                     p_sems.at[1, dz, p], plane_peers[dy, dx])
    far = {}
    final = None
    for dz in list(range(1, n_hi)) + [0]:
        total = far_total[dz]
        for p in range(len(g.plane)):
            planes[dz, p].wait()
            total = total + p_recv[dz, p].astype(F32)
        if dz:
            f_send[dz] = total.astype(BF16)
            far[dz] = send(f_send.at[dz], f_recv.at[dz], f_sems.at[0, dz], f_sems.at[1, dz],
                           g.at(step(g.hi, dz, n_hi), g.lo, g.x, g.core))
        else:
            final = total
    for dz in range(1, n_hi):
        far[dz].wait()
        final = final + f_recv[dz].astype(F32)
    out_ref[...] = (gathered[mine].astype(F32) + final).astype(out_ref.dtype)


def tail(grid, merged, tokens, mlp_gain, w_out, w_up, w_down):
    g = grid
    batch, size = tokens.shape
    n_dev = g.n_kv * g.n_tp
    n_plane = max(1, len(g.plane))
    vmem = pl.BlockSpec(memory_space=pltpu.VMEM)
    hbm = pl.BlockSpec(memory_space=pl.ANY)
    dma = pltpu.SemaphoreType.DMA
    block = (batch, size)
    return pl.pallas_call(
        functools.partial(tail_kernel, g),
        out_shape=jax.ShapeDtypeStruct(block, BF16),
        in_specs=[vmem] * 3 + [hbm] * 3,
        out_specs=vmem,
        scratch_shapes=[
            pltpu.VMEM(w_out.shape, BF16),
            pltpu.VMEM(w_up.shape, BF16),
            pltpu.VMEM(w_down.shape, BF16),
            pltpu.VMEM((g.n_kv,) + merged.shape, BF16),
            pltpu.VMEM((g.n_tp,) + block, F32),
            pltpu.VMEM((g.n_tp,) + block, BF16),
            pltpu.VMEM((g.n_tp,) + block, BF16),
            pltpu.VMEM((n_dev,) + block, BF16),
            pltpu.VMEM((batch, w_up.shape[1]), F32),
            pltpu.VMEM((g.n_kv, g.n_x) + block, F32),
            pltpu.VMEM((g.n_kv, g.n_x) + block, BF16),
            pltpu.VMEM((g.n_kv, g.n_x) + block, BF16),
            pltpu.VMEM((g.n_hi, n_plane) + block, BF16),
            pltpu.VMEM((g.n_hi, n_plane) + block, BF16),
            pltpu.VMEM((g.n_hi,) + block, F32),
            pltpu.VMEM((g.n_hi,) + block, BF16),
            pltpu.VMEM((g.n_hi,) + block, BF16),
            dma((3,)),
            dma,
            dma((2, g.n_kv)),
            dma((2, g.n_tp)),
            dma((2, g.n_hi)),
            dma((2, g.n_hi, n_plane)),
            dma((2, g.n_kv * g.n_x)),
            dma((2, g.n_kv)),
            dma((2, g.n_hi, n_plane)),
            dma((2, g.n_hi)),
        ],
        compiler_params=pltpu.CompilerParams(
            collective_id=1, has_side_effects=True, vmem_limit_bytes=VMEM_BYTES
        ),
        name="tail",
    )(merged, tokens, mlp_gain.reshape(n_dev, 1, size), w_out, w_up, w_down)


def head_norm(values):
    return values * lax.rsqrt(jnp.sum(values * values, axis=-1, keepdims=True) + EPSILON)


def local(
    n_kv, n_tp,
    tokens, mix_gain, w_query, w_key, w_value, w_gate, w_beta, w_decay, decay_rate, out_gain,
    state, w_out, mlp_gain, w_up, w_down,
):
    rows, heads, size, _ = state.shape
    all_heads = w_beta.shape[1]
    features = w_query.shape[0] * n_kv
    rate_width = 2 * all_heads
    lanes = -(-(rate_width + 1) // 128) * 128
    w_rates = jnp.concatenate(
        [w_beta, w_decay, jnp.zeros((w_beta.shape[0], lanes - rate_width), w_beta.dtype)], axis=1
    )
    raw, rates = project(
        Grid(n_kv, n_tp), tokens, mix_gain, (w_query, w_key, w_value, w_gate), w_rates, rate_width
    )
    row_scale = lax.rsqrt(rates[:, rate_width : rate_width + 1] / features + EPSILON)
    raw = (raw * row_scale).reshape(4, rows, heads, size)
    query = head_norm(jax.nn.silu(raw[0])) * size ** (-0.5)
    key = head_norm(jax.nn.silu(raw[1]))
    value = jax.nn.silu(raw[2])
    gate = jax.nn.silu(raw[3])
    rates = rates * row_scale
    head_start = lax.axis_index("tp") * heads
    beta = jax.nn.sigmoid(lax.dynamic_slice_in_dim(rates, head_start, heads, 1))
    decay_raw = lax.dynamic_slice_in_dim(rates, all_heads + head_start, heads, 1)
    decay = jnp.exp(-decay_rate[None, :] * jax.nn.softplus(decay_raw))
    new_state, merged = update_state(state, key, query, value, gate, decay, beta, out_gain)
    merged = merged.reshape(rows, heads * size).astype(BF16)
    mixed = tail(Grid(n_kv, n_tp), merged, tokens, mlp_gain, w_out, w_up, w_down)
    return (mixed, new_state)


def solution(mesh):
    placed = (
        P(None, ("kv", "tp")),
        P("kv"),
        P("kv", "tp"),
        P("kv", "tp"),
        P("kv", "tp"),
        P("kv", "tp"),
        P("kv", None),
        P("kv", None),
        P("tp"),
        P(),
        P("kv", "tp", None, None),
        P("tp", "kv"),
        P(),
        P(None, ("kv", "tp")),
        P(("kv", "tp"), None),
    )
    return jax.shard_map(
        functools.partial(local, mesh.shape["kv"], mesh.shape["tp"]),
        mesh=mesh,
        in_specs=placed,
        out_specs=(P(None, ("kv", "tp")), P("kv", "tp", None, None)),
        check_vma=False,
    )
```

time: 619 us -> 99.8 us (0.16)
  waiting for transfers between devices: 499 us -> 0 us
  Pallas kernels: 0 us -> 84 us
  blocking collectives: 59.7 us -> 0 us
  matrix products: 28.8 us -> 0 us
  between operations: 15.1 us -> 0.73 us
    reduce_scatter x7 -> x0, waiting for transfers between devices: 449 us -> none  [the longest x1 138 us: local(): lax.psum_scatter(partial_mlp, ('kv', 'tp'), scatter_dimension=1, tiled=True)]
    pallas_call x0 -> x3, Pallas kernels: none -> 84 us  [the longest x1 41.9 us: tail(): pl.pallas_call(functools.partial(tail_kernel, g), out_shape=jax.ShapeDtyp...]
    all_gather x1 -> x0, waiting for transfers between devices: 50.4 us -> none  [local(): whole_rows = lax.all_gather(residual, ('kv', 'tp'), axis=1, tiled=True)]
    all_gather x2 -> x0, blocking collectives: 37.6 us -> none  [the longest x1 30.7 us: local(): lax.all_gather(merged, 'kv', axis=0, tiled=True)]
    dot_general x9 -> x0, matrix products: 28.8 us -> none  [the longest x1 7.72 us: local(): jnp.einsum('bhkv,bhk->bhv', faded, key, precision=lax.Precision.HIGHEST)]
    unnamed x1 -> x0, blocking collectives: 22.1 us -> none
  transfers between devices with their start and end apart: 8 -> 0, of which waited for: 8 -> 0; matrix products, arithmetic and copies ran while one was open for 1% -> 0% of each run, Pallas kernels for 0% -> 0%
where the time goes in v1:
time: 99.8 us; the launch traced here: 98.9 us
  Pallas kernels  84 us (84%)
  local copies, waits for them, and re-layouts  8.01 us (8%)
  other arithmetic  6.14 us (6%)
    pallas_call x1, Pallas kernels, tail(): pl.pallas_call(functools.partial(tail_kernel, g), out_shape=jax.ShapeDtyp...  41.9 us
    pallas_call x1, Pallas kernels, project(): pl.pallas_call(functools.partial(project_kernel, g, rate_width), out_shap...  27 us
    pallas_call x1, Pallas kernels, update_state(): pl.pallas_call(state_kernel, grid=(rows,), out_shape=(jax.ShapeDtypeStruc...  15.1 us
    unnamed x4, local copies, waits for them, and re-layouts  3.71 us

profile of v1, /device:TPU:0, one launch (start us, length us, event | category | flops | bytes accessed | tf_op | source)
XLA Modules:
  0.0 98.9 jit_solution(10693883989071492619)
XLA Ops:
  0.6 0.7 neg.36
  1.3 0.1 pad.2.clone
  1.4 0.9 copy.21
  2.2 0.9 copy.22
  3.1 0.8 maximum_maximum_fusion.wr_ref
  3.9 27.0 %project.1 = (f32[4,16,768]{2,1,0:T(8,128)}, f32[16,128]{1,0:T(8,128)}) custom-call(bf16[128,128]{1,0:T(8,128)(2,1)} %tok_ref.3, f32[4,1,128]{2,1,0:T(1,128)} %bitcast.14, bf16[512,768]{1,0:T(8,128)(2,1)} %wq_ref.1, bf16[512,768]{1,0:T(8,128)(2,1)} %wk_ref.1, bf16[512,768]{1,0:T(8,128)(2,1)} %wv_ref.1, bf16[512,768]{1,0:T(8,128)(2,1)} %wg_ref.1, ...), custom_call_target="tpu_custom_call" | custom-call | tf_op jit(solution)/shard_map/project/pallas_call | solution.py:157
  30.9 0.9 rsqrt_reduce_fusion
  31.8 0.8 broadcast_multiply_fusion.1
  32.5 1.0 %broadcast_multiply_fusion = f32[4,16,768]{2,1,0:T(8,128)S(1)} fusion(f32[4,16,768]{2,1,0:T(8,128)} %get-tuple-element.6, f32[16]{0:T(128)S(1)} %rsqrt_reduce_fusion), kind=kLoop, calls=%fused_computation.1 | loop fusion | flops 49152 | bytes 393280 | tf_op jit(solution)/shard_map/mul | solution.py:508
  33.6 0.1 add_divide_fusion
  33.7 0.7 broadcast_in_dim.8.beta_ref
  34.4 0.1 multiply_reduce_fusion
  34.5 0.1 multiply_bitcast_fusion
  34.7 0.1 multiply_reduce_fusion.1
  34.8 0.1 multiply_bitcast_fusion.1
  34.9 0.7 broadcast_in_dim.7.decay_ref
  35.6 0.7 divide_multiply_fusion
  36.3 1.4 %copy.23.kt_ref = f32[16,128,6]{2,1,0:T(8,128)} copy(f32[16,128,6]{1,2,0:T(8,128)S(1)} %multiply_bitcast_fusion.1) | data formatting | bytes 98304 | tf_op jit(solution)/shard_map/transpose | solution.py:225
  37.6 1.4 %copy.24.qt_ref = f32[16,128,6]{2,1,0:T(8,128)} copy(f32[16,128,6]{1,2,0:T(8,128)S(1)} %multiply_bitcast_fusion) | data formatting | bytes 98304 | tf_op jit(solution)/shard_map/transpose | solution.py:226
  39.0 15.1 %state.1 = (f32[16,6,128,128]{3,2,1,0:T(8,128)}, f32[16,6,128]{2,1,0:T(8,128)}) custom-call(f32[16,6,128,128]{3,2,1,0:T(8,128)} %s_ref.1, f32[16,128,6]{2,1,0:T(8,128)} %copy.23.kt_ref, f32[16,128,6]{2,1,0:T(8,128)} %copy.24.qt_ref, f32[16,6,128]{2,1,0:T(8,128)} %get-tuple-element.17.value_ref, f32[16,6,128]{2,1,0:T(8,128)} %get-tuple-element.16.gate_ref, ...), custom_call_target="tpu_custom_call" | custom-call | tf_op jit(solution)/shard_map/state/pallas_call | solution.py:211
  54.2 0.8 convert_element_type.5
  55.0 0.6 copy.27
  55.6 41.9 %tail.1 = bf16[128,128]{1,0:T(8,128)(2,1)} custom-call(bf16[16,768]{1,0:T(8,128)(2,1)} %bitcast.12, bf16[128,128]{1,0:T(8,128)(2,1)} %tok_ref.3, f32[32,1,128]{2,1,0:T(1,128)} %bitcast.13, bf16[768,512]{1,0:T(8,128)(2,1)} %wout_hbm.1, bf16[4096,512]{1,0:T(8,128)(2,1)} %wup_hbm.1, bf16[512,4096]{1,0:T(8,128)(2,1)} %wdown_hbm.1), custom_call_target="tpu_custom_call" | custom-call | tf_op jit(solution)/shard_map/tail/pallas_call | solution.py:446
  97.5 1.4 %copy.29 = bf16[128,128]{1,0:T(8,128)(2,1)} copy(bf16[128,128]{1,0:T(8,128)(2,1)} %tail.1) | data formatting | bytes 65536
  (8 shorter events, 0.1 us)

commit v2 on v1

v2 whole, which is shorter than its diff:
```python
import functools
import math

import jax
import jax.numpy as jnp
from jax import lax
from jax.experimental import pallas as pl
from jax.experimental.pallas import tpu as pltpu
from jax.sharding import PartitionSpec as P

EPSILON = 1e-06
CORES = 2
VMEM_BYTES = 60 * 2**20
BF16 = jnp.bfloat16
F32 = jnp.float32


class Grid:
    def __init__(self, n_kv, n_tp):
        self.n_kv, self.n_tp = n_kv, n_tp
        low = max(f for f in range(1, math.isqrt(n_kv) + 1) if n_kv % f == 0)
        self.n_lo, self.n_hi = low, n_kv // low
        self.n_core = CORES if n_tp % CORES == 0 else 1
        self.n_x = n_tp // self.n_core
        self.plane = [
            (dy, dx) for dy in range(self.n_lo) for dx in range(self.n_x) if (dy, dx) != (0, 0)
        ]

    def locate(self):
        self.kv, self.tp = lax.axis_index("kv"), lax.axis_index("tp")
        self.hi, self.lo = self.kv // self.n_lo, lax.rem(self.kv, self.n_lo)
        self.x, self.core = self.tp // self.n_core, lax.rem(self.tp, self.n_core)

    def at(self, hi, lo, x, core):
        return (hi * self.n_lo + lo, x * self.n_core + core)


def step(index, offset, size):
    return lax.rem(index + (offset % size), size) if offset % size else index


def send(src, dst, send_sem, recv_sem, device):
    copy = pltpu.make_async_remote_copy(
        src_ref=src,
        dst_ref=dst,
        send_sem=send_sem,
        recv_sem=recv_sem,
        device_id=device,
        device_id_type=pl.DeviceIdType.MESH,
    )
    copy.start()
    return copy


def silu(values):
    return values / (1.0 + jnp.exp(-values))


def layer_kernel(
    grid, all_heads, lane_gap, features,
    tok_ref, mix_ref, wb_ref, wd_ref, rate_ref, out_gain_ref, gain_ref,
    wk_hbm, wq_hbm, wv_hbm, wg_hbm, state_hbm, wout_hbm, wup_hbm, wdown_hbm,
    out_ref, key_ref, change_ref, decay_ref,
    cols, w_mix, w_rates, part, rate_part, rate_recv,
    near_send, near_recv, far_total, far_send, far_recv,
    state, query_buf, value_buf, gate_buf, recalled, echoed,
    wout, wup, wdown, mg, rs_own, rs_send, rs_recv, gathered, acc,
    y_own, y_send, y_recv, p_send, p_recv, last_total, f_send, f_recv,
    mix_load_sems, load_sems, own_sem, tok_sems, rate_sems, near_sems, far_sems,
    mg_sems, rs_sems, ghi_sems, gpl_sems, gco_sems, y_sems, p_sems, f_sems,
):
    g = grid
    g.locate()
    n_kv, n_tp, n_lo, n_hi, n_x = g.n_kv, g.n_tp, g.n_lo, g.n_hi, g.n_x
    batch, size = tok_ref.shape
    heads, rows, head_size = key_ref.shape
    own_cols = pltpu.make_async_copy(tok_ref, cols.at[g.tp], own_sem)
    own_cols.start()
    kv_peers = [(step(g.kv, k, n_kv), g.tp) for k in range(1, n_kv)]
    tp_peers = [(g.kv, step(g.tp, k, n_tp)) for k in range(1, n_tp)]
    plane_peers = {
        (dy, dx): g.at(g.hi, step(g.lo, dy, n_lo), step(g.x, dx, n_x), g.core)
        for dy, dx in g.plane
    }
    barrier = pltpu.get_barrier_semaphore()
    everyone = kv_peers + tp_peers + [plane_peers[d] for d in g.plane if d[0] and d[1]]
    for peer in everyone:
        pl.semaphore_signal(barrier, inc=1, device_id=peer, device_id_type=pl.DeviceIdType.MESH)
    mix_loads = [
        pltpu.make_async_copy(w, w_mix.at[c], mix_load_sems.at[c])
        for c, w in enumerate((wk_hbm, wq_hbm, wv_hbm, wg_hbm))
    ]
    loads = [
        pltpu.make_async_copy(a, b, load_sems.at[i])
        for i, (a, b) in enumerate(
            ((wout_hbm, wout), (wup_hbm, wup), (wdown_hbm, wdown), (state_hbm, state))
        )
    ]
    for load in mix_loads + [loads[3]] + loads[:3]:
        load.start()
    w_rates[...] = jnp.zeros_like(w_rates)
    w_rates[0:all_heads, :] = wb_ref[...]
    w_rates[lane_gap : lane_gap + all_heads, :] = wd_ref[...]
    pl.semaphore_wait(barrier, len(everyone))

    started = [
        send(tok_ref, cols.at[g.tp], tok_sems.at[0, k], tok_sems.at[1, k], tp_peers[k - 1])
        for k in range(1, n_tp)
    ]
    own_cols.wait()
    for copy in started:
        copy.wait()
    blocks = [cols[i].astype(F32) for i in range(n_tp)]
    squares = sum(jnp.sum(b * b, axis=1, keepdims=True) for b in blocks)
    normed = [(blocks[i] * mix_ref[i]).astype(BF16) for i in range(n_tp)]
    if size % 128 == 0:
        normed = [jnp.concatenate(normed, axis=1)]
    depth = normed[0].shape[1]

    rates = sum(
        lax.dot_general(
            normed[i], w_rates[:, i * depth : (i + 1) * depth], (((1,), (1,)), ((), ())),
            preferred_element_type=F32,
        )
        for i in range(len(normed))
    )
    lane = lax.broadcasted_iota(jnp.int32, rates.shape, 1)
    rates = jnp.where(lane == 2 * lane_gap, squares, rates)
    rate_part[...] = rates.reshape(n_kv, rows, rates.shape[1])
    rate_copies = [
        send(rate_part.at[step(g.kv, k, n_kv)], rate_recv.at[k], rate_sems.at[0, k],
             rate_sems.at[1, k], kv_peers[k - 1])
        for k in range(1, n_kv)
    ]
    near = {}
    for c in range(4):
        mix_loads[c].wait()
        value = sum(
            jnp.dot(normed[i], w_mix[c, i * depth : (i + 1) * depth, :],
                    preferred_element_type=F32)
            for i in range(len(normed))
        ).reshape(n_kv, rows, w_mix.shape[2])
        part[c] = value
        for lo in range(n_lo):
            for hi in range(n_hi):
                near_send[c, lo, hi] = value[hi * n_lo + lo].astype(BF16)
        for k in range(1, n_lo):
            lo = step(g.lo, k, n_lo)
            near[c, k] = send(near_send.at[c, lo], near_recv.at[c, k], near_sems.at[0, c, k],
                              near_sems.at[1, c, k], (g.hi * n_lo + lo, g.tp))
    far = {}
    for c in range(4):
        for k in range(1, n_lo):
            near[c, k].wait()
        for d in list(range(1, n_hi)) + [0]:
            hi = step(g.hi, d, n_hi)
            total = part[c, hi * n_lo + g.lo]
            for k in range(1, n_lo):
                total = total + near_recv[c, k, hi].astype(F32)
            if d == 0:
                far_total[c] = total
            else:
                far_send[c, d] = total.astype(BF16)
                far[c, d] = send(far_send.at[c, d], far_recv.at[c, d], far_sems.at[0, c, d],
                                 far_sems.at[1, c, d], (hi * n_lo + g.lo, g.tp))
    for copy in rate_copies:
        copy.wait()
    rates = rate_part[g.kv]
    for k in range(1, n_kv):
        rates = rates + rate_recv[k]
    lane = lax.broadcasted_iota(jnp.int32, rates.shape, 1)

    def pick(index):
        return jnp.sum(jnp.where(lane == index, rates, 0.0), axis=1, keepdims=True)

    row_scale = lax.rsqrt(pick(2 * lane_gap) / features + EPSILON)

    def arrived(c):
        total = far_total[c]
        for d in range(1, n_hi):
            far[c, d].wait()
            total = total + far_recv[c, d].astype(F32)
        return silu(total * row_scale)

    def unit(values):
        return values * lax.rsqrt(jnp.sum(values * values, axis=1, keepdims=True) + EPSILON)

    def of_head(values, h):
        return values[:, h * head_size : (h + 1) * head_size]

    keys = arrived(0)
    for h in range(heads):
        key_ref[h] = unit(of_head(keys, h))
    queries = arrived(1)
    for h in range(heads):
        query_buf[h] = unit(of_head(queries, h)) * head_size ** (-0.5)
    loads[3].wait()

    @pl.loop(0, heads)
    def _(h):
        tall_key, tall_query = key_ref[h].T, query_buf[h].T
        for r in range(rows):
            block = state[r, h]
            recalled[h, r : r + 1, :] = jnp.sum(
                block * tall_key[:, r : r + 1], axis=0, keepdims=True
            )
            echoed[h, r : r + 1, :] = jnp.sum(
                block * tall_query[:, r : r + 1], axis=0, keepdims=True
            )

    value_buf[...] = arrived(2)
    gate_buf[...] = arrived(3)
    head_start = g.tp * heads
    own_merged = mg.at[g.kv]
    for h in range(heads):
        beta = 1.0 / (1.0 + jnp.exp(-(pick(head_start + h) * row_scale)))
        decay_raw = pick(head_start + (lane_gap + h)) * row_scale
        softplus = jnp.maximum(decay_raw, 0.0) + jnp.log1p(jnp.exp(-jnp.abs(decay_raw)))
        decay = jnp.exp(-(rate_ref[:, h : h + 1] * softplus))
        change = beta * (of_head(value_buf, h) - decay * recalled[h])
        overlap = jnp.sum(key_ref[h] * query_buf[h], axis=1, keepdims=True)
        readout = decay * echoed[h] + overlap * change
        change_ref[h] = change
        decay_ref[h] = jnp.broadcast_to(decay, change.shape)
        scaled = (
            readout
            * lax.rsqrt(jnp.mean(readout * readout, axis=1, keepdims=True) + EPSILON)
            * out_gain_ref[...]
        )
        own_merged[:, h * head_size : (h + 1) * head_size] = (
            scaled * of_head(gate_buf, h)
        ).astype(BF16)

    started = [
        send(own_merged, own_merged, mg_sems.at[0, k], mg_sems.at[1, k], kv_peers[k - 1])
        for k in range(1, n_kv)
    ]
    loads[0].wait()
    for k in range(1, n_kv):
        started[k - 1].wait_send()
        pltpu.make_async_remote_copy(
            src_ref=own_merged, dst_ref=mg.at[step(g.kv, -k, n_kv)], send_sem=mg_sems.at[0, k],
            recv_sem=mg_sems.at[1, k], device_id=kv_peers[k - 1],
            device_id_type=pl.DeviceIdType.MESH,
        ).wait_recv()
    partial = jnp.dot(
        mg[...].reshape(n_kv * rows, mg.shape[2]), wout[...], preferred_element_type=F32
    )
    for t in range(n_tp):
        block = partial[:, t * size : (t + 1) * size]
        rs_own[t] = block
        rs_send[t] = block.astype(BF16)
    started = [
        send(rs_send.at[step(g.tp, k, n_tp)], rs_recv.at[k], rs_sems.at[0, k], rs_sems.at[1, k],
             tp_peers[k - 1])
        for k in range(1, n_tp)
    ]
    branch = rs_own[g.tp]
    for k in range(1, n_tp):
        started[k - 1].wait()
        branch = branch + rs_recv[k].astype(F32)
    residual = (tok_ref[...].astype(F32) + branch).astype(BF16)

    def index(dz, dy, dx, core):
        kv, tp = g.at(step(g.hi, -dz, n_hi), step(g.lo, -dy, n_lo), step(g.x, -dx, n_x), core)
        return kv * n_tp + tp

    mine = index(0, 0, 0, g.core)
    gathered[mine] = residual
    pending = []
    sibling = None if g.n_core == 1 else g.at(g.hi, g.lo, g.x, 1 - g.core)

    def to_sibling(dz, dy, dx):
        if sibling is None:
            return
        place = gathered.at[index(dz, dy, dx, g.core)]
        slot = (dz * n_lo + dy) * n_x + dx
        send(place, place, gco_sems.at[0, slot], gco_sems.at[1, slot], sibling)
        other = gathered.at[index(dz, dy, dx, 1 - g.core)]
        pending.append((place, other, gco_sems.at[0, slot], gco_sems.at[1, slot]))

    def wait_for(src, dst, send_sem, recv_sem, device):
        copy = pltpu.make_async_remote_copy(
            src_ref=src, dst_ref=dst, send_sem=send_sem, recv_sem=recv_sem,
            device_id=device, device_id_type=pl.DeviceIdType.MESH,
        )
        copy.wait_recv()

    sent = []
    own = gathered.at[mine]
    for dz in range(1, n_hi):
        peer = g.at(step(g.hi, dz, n_hi), g.lo, g.x, g.core)
        sent.append(send(own, own, ghi_sems.at[0, dz], ghi_sems.at[1, dz], peer))
    for dz in range(n_hi):
        place = gathered.at[index(dz, 0, 0, g.core)]
        if dz:
            wait_for(own, place, ghi_sems.at[0, dz], ghi_sems.at[1, dz],
                     g.at(step(g.hi, dz, n_hi), g.lo, g.x, g.core))
        for p, d in enumerate(g.plane):
            sent.append(send(place, place, gpl_sems.at[0, dz, p], gpl_sems.at[1, dz, p],
                             plane_peers[d]))
        to_sibling(dz, 0, 0)
    for dz in range(n_hi):
        for p, (dy, dx) in enumerate(g.plane):
            place = gathered.at[index(dz, dy, dx, g.core)]
            wait_for(own, place, gpl_sems.at[0, dz, p], gpl_sems.at[1, dz, p],
                     plane_peers[dy, dx])
            to_sibling(dz, dy, dx)
    for copy in sent:
        copy.wait_send()
    for place, other, send_sem, recv_sem in pending:
        copy = pltpu.make_async_remote_copy(
            src_ref=place, dst_ref=other, send_sem=send_sem, recv_sem=recv_sem,
            device_id=sibling, device_id_type=pl.DeviceIdType.MESH,
        )
        copy.wait_recv()
        copy.wait_send()

    n_dev = n_kv * n_tp

    def add_squares(i, total):
        block = gathered[i].astype(F32)
        return total + jnp.sum(block * block, axis=1, keepdims=True)

    squares = lax.fori_loop(0, n_dev, add_squares, jnp.zeros((batch, 1), F32))
    scale = lax.rsqrt(squares / features + EPSILON)
    group = n_tp if size % 128 == 0 else 1
    loads[1].wait()
    acc[...] = jnp.zeros_like(acc)

    @pl.loop(0, n_dev // group)
    def _(i):
        parts = [
            (gathered[i * group + j].astype(F32) * scale * gain_ref[i * group + j]).astype(BF16)
            for j in range(group)
        ]
        block = parts[0] if group == 1 else jnp.concatenate(parts, axis=1)
        depth = group * size
        acc[...] += jnp.dot(
            block, wup[pl.ds(pl.multiple_of(i * depth, depth), depth), :],
            preferred_element_type=F32,
        )

    hidden = jnp.square(jnp.maximum(acc[...], 0.0)).astype(BF16)
    loads[2].wait()
    width = n_tp * size

    def down(j):
        columns = pl.ds(pl.multiple_of(j * width, width), width)
        value = jnp.dot(hidden, wdown[:, columns], preferred_element_type=F32)
        for x in range(n_x):
            pair = [
                value[:, (x * g.n_core + c) * size : (x * g.n_core + c + 1) * size]
                for c in range(g.n_core)
            ]
            if g.n_core == 1:
                y_own[j, x] = pair[0]
            else:
                y_own[j, x] = jnp.where(g.core == 0, pair[0], pair[1])
                y_send[j, x] = jnp.where(g.core == 0, pair[1], pair[0]).astype(BF16)

    order = [(dz, dy) for dz in list(range(1, n_hi)) + [0] for dy in range(n_lo)]

    def kv_of(dz, dy):
        return step(g.hi, dz, n_hi) * n_lo + step(g.lo, dy, n_lo)

    swaps = {}
    for s, (dz, dy) in enumerate(order):
        j = kv_of(dz, dy)
        down(j)
        if sibling is not None:
            swaps[dz, dy] = send(y_send.at[j], y_recv.at[j], y_sems.at[0, s], y_sems.at[1, s],
                                 sibling)
    planes = {}
    for dz, dy in order:
        j = kv_of(dz, dy)
        if sibling is not None:
            swaps[dz, dy].wait()
        for dx in range(n_x):
            x = step(g.x, dx, n_x)
            total = y_own[j, x]
            if sibling is not None:
                total = total + y_recv[j, x].astype(F32)
            if (dy, dx) == (0, 0):
                last_total[dz] = total
            else:
                p = g.plane.index((dy, dx))
                p_send[dz, p] = total.astype(BF16)
                planes[dz, p] = send(p_send.at[dz, p], p_recv.at[dz, p], p_sems.at[0, dz, p],
                                     p_sems.at[1, dz, p], plane_peers[dy, dx])
    last = {}
    final = None
    for dz in list(range(1, n_hi)) + [0]:
        total = last_total[dz]
        for p in range(len(g.plane)):
            planes[dz, p].wait()
            total = total + p_recv[dz, p].astype(F32)
        if dz:
            f_send[dz] = total.astype(BF16)
            last[dz] = send(f_send.at[dz], f_recv.at[dz], f_sems.at[0, dz], f_sems.at[1, dz],
                           g.at(step(g.hi, dz, n_hi), g.lo, g.x, g.core))
        else:
            final = total
    for dz in range(1, n_hi):
        last[dz].wait()
        final = final + f_recv[dz].astype(F32)
    out_ref[...] = (gathered[mine].astype(F32) + final).astype(out_ref.dtype)


def layer(grid, tokens, mix_gain, weights, w_beta, w_decay, decay_rate, out_gain, state, w_out,
          mlp_gain, w_up, w_down):
    g = grid
    batch, size = tokens.shape
    n_dev = g.n_kv * g.n_tp
    rows, heads, head_size, _ = state.shape
    depth, width = weights[0].shape
    all_heads = w_beta.shape[1]
    lane_gap = -(-all_heads // 32) * 32
    lanes = -(-(2 * lane_gap + 1) // 128) * 128
    n_plane = max(1, len(g.plane))
    vmem = pl.BlockSpec(memory_space=pltpu.VMEM)
    hbm = pl.BlockSpec(memory_space=pl.ANY)
    dma = pltpu.SemaphoreType.DMA
    block = (batch, size)
    per_head = (heads, rows, head_size)
    return pl.pallas_call(
        functools.partial(layer_kernel, g, all_heads, lane_gap, n_dev * size),
        out_shape=(
            jax.ShapeDtypeStruct(block, BF16),
            jax.ShapeDtypeStruct(per_head, F32),
            jax.ShapeDtypeStruct(per_head, F32),
            jax.ShapeDtypeStruct(per_head, F32),
        ),
        in_specs=[vmem] * 7 + [hbm] * 8,
        out_specs=(vmem,) * 4,
        scratch_shapes=[
            pltpu.VMEM((g.n_tp,) + block, BF16),
            pltpu.VMEM((4, depth, width), BF16),
            pltpu.VMEM((lanes, depth), BF16),
            pltpu.VMEM((4, g.n_kv, rows, width), F32),
            pltpu.VMEM((g.n_kv, rows, lanes), F32),
            pltpu.VMEM((g.n_kv, rows, lanes), F32),
            pltpu.VMEM((4, g.n_lo, g.n_hi, rows, width), BF16),
            pltpu.VMEM((4, g.n_lo, g.n_hi, rows, width), BF16),
            pltpu.VMEM((4, rows, width), F32),
            pltpu.VMEM((4, g.n_hi, rows, width), BF16),
            pltpu.VMEM((4, g.n_hi, rows, width), BF16),
            pltpu.VMEM(state.shape, F32),
            pltpu.VMEM(per_head, F32),
            pltpu.VMEM((rows, width), F32),
            pltpu.VMEM((rows, width), F32),
            pltpu.VMEM(per_head, F32),
            pltpu.VMEM(per_head, F32),
            pltpu.VMEM(w_out.shape, BF16),
            pltpu.VMEM(w_up.shape, BF16),
            pltpu.VMEM(w_down.shape, BF16),
            pltpu.VMEM((g.n_kv, rows, width), BF16),
            pltpu.VMEM((g.n_tp,) + block, F32),
            pltpu.VMEM((g.n_tp,) + block, BF16),
            pltpu.VMEM((g.n_tp,) + block, BF16),
            pltpu.VMEM((n_dev,) + block, BF16),
            pltpu.VMEM((batch, w_up.shape[1]), F32),
            pltpu.VMEM((g.n_kv, g.n_x) + block, F32),
            pltpu.VMEM((g.n_kv, g.n_x) + block, BF16),
            pltpu.VMEM((g.n_kv, g.n_x) + block, BF16),
            pltpu.VMEM((g.n_hi, n_plane) + block, BF16),
            pltpu.VMEM((g.n_hi, n_plane) + block, BF16),
            pltpu.VMEM((g.n_hi,) + block, F32),
            pltpu.VMEM((g.n_hi,) + block, BF16),
            pltpu.VMEM((g.n_hi,) + block, BF16),
            dma((4,)),
            dma((4,)),
            dma,
            dma((2, g.n_tp)),
            dma((2, g.n_kv)),
            dma((2, 4, g.n_lo)),
            dma((2, 4, g.n_hi)),
            dma((2, g.n_kv)),
            dma((2, g.n_tp)),
            dma((2, g.n_hi)),
            dma((2, g.n_hi, n_plane)),
            dma((2, g.n_kv * g.n_x)),
            dma((2, g.n_kv)),
            dma((2, g.n_hi, n_plane)),
            dma((2, g.n_hi)),
        ],
        compiler_params=pltpu.CompilerParams(
            collective_id=0, has_side_effects=True, vmem_limit_bytes=VMEM_BYTES
        ),
        name="layer",
    )(
        tokens, mix_gain.reshape(g.n_tp, 1, size), w_beta.T, w_decay.T,
        decay_rate.reshape(1, heads), out_gain.reshape(1, head_size),
        mlp_gain.reshape(n_dev, 1, size), *weights, state, w_out, w_up, w_down,
    )


def state_kernel(state_ref, key_ref, change_ref, decay_ref, new_ref):
    tall = key_ref[0].T
    for r in range(state_ref.shape[0]):
        row = slice(r, r + 1)
        new_ref[r, 0] = (
            state_ref[r, 0] * decay_ref[0, row, :] + tall[:, row] * change_ref[0, row, :]
        )


def write_state(state, key, change, decay):
    rows, heads, size, _ = state.shape
    whole = pl.BlockSpec((rows, 1, size, size), lambda i: (0, i, 0, 0))
    small = pl.BlockSpec((1, rows, size), lambda i: (i, 0, 0))
    return pl.pallas_call(
        state_kernel,
        grid=(heads,),
        out_shape=jax.ShapeDtypeStruct(state.shape, F32),
        in_specs=[whole, small, small, small],
        out_specs=whole,
        compiler_params=pltpu.CompilerParams(dimension_semantics=("arbitrary",)),
        name="state",
    )(state, key, change, decay)


def local(
    n_kv, n_tp,
    tokens, mix_gain, w_query, w_key, w_value, w_gate, w_beta, w_decay, decay_rate, out_gain,
    state, w_out, mlp_gain, w_up, w_down,
):
    mixed, key, change, decay = layer(
        Grid(n_kv, n_tp), tokens, mix_gain, (w_key, w_query, w_value, w_gate), w_beta, w_decay,
        decay_rate, out_gain, state, w_out, mlp_gain, w_up, w_down,
    )
    return (mixed, write_state(state, key, change, decay))


def solution(mesh):
    placed = (
        P(None, ("kv", "tp")),
        P("kv"),
        P("kv", "tp"),
        P("kv", "tp"),
        P("kv", "tp"),
        P("kv", "tp"),
        P("kv", None),
        P("kv", None),
        P("tp"),
        P(),
        P("kv", "tp", None, None),
        P("tp", "kv"),
        P(),
        P(None, ("kv", "tp")),
        P(("kv", "tp"), None),
    )
    return jax.shard_map(
        functools.partial(local, mesh.shape["kv"], mesh.shape["tp"]),
        mesh=mesh,
        in_specs=placed,
        out_specs=(P(None, ("kv", "tp")), P("kv", "tp", None, None)),
        check_vma=False,
    )
```

time: 99.8 us -> 74.7 us (0.75)
  Pallas kernels: 84 us -> 73.1 us
  local copies, waits for them, and re-layouts: 8.01 us -> 0.62 us
  other arithmetic: 6.14 us -> 0 us
    pallas_call x3 -> x2, Pallas kernels: 84 us -> 73.1 us  [the longest x1 65 us: layer(): pl.pallas_call(functools.partial(layer_kernel, g, all_heads, lane_gap, n_...]
    unnamed x4 -> x3, local copies, waits for them, and re-layouts: 3.71 us -> 0.62 us
    transpose x2 -> x0, local copies, waits for them, and re-layouts: 2.76 us -> none  [the longest x1 1.4 us: update_state(): jnp.swapaxes(query, 1, 2)]
    mul x3 -> x0, other arithmetic: 2.49 us -> none  [the longest x1 1.01 us: local(): raw = (raw * row_scale).reshape(4, rows, heads, size)]
    broadcast_in_dim x3 -> x0, local copies, waits for them, and re-layouts: 1.41 us -> none  [the longest x1 0.7 us: update_state(): jnp.broadcast_to(beta[:, :, None], value.shape)]
where the time goes in v2:
time: 74.7 us; the launch traced here: 74.4 us
  Pallas kernels  73.1 us (98%)
    pallas_call x1, Pallas kernels, layer(): pl.pallas_call(functools.partial(layer_kernel, g, all_heads, lane_gap, n_...  65 us
    pallas_call x1, Pallas kernels, write_state(): pl.pallas_call(state_kernel, grid=(heads,), out_shape=jax.ShapeDtypeStruc...  8.14 us

profile of v2, /device:TPU:0, one launch (start us, length us, event | category | flops | bytes accessed | tf_op | source)
XLA Modules:
  0.0 74.4 jit_solution(9456978975460050835)
XLA Ops:
  0.6 65.0 %layer.1 = (bf16[128,128]{1,0:T(8,128)(2,1)}, f32[6,16,128]{2,1,0:T(8,128)}, f32[6,16,128]{2,1,0:T(8,128)}, f32[6,16,128]{2,1,0:T(8,128)}) custom-call(bf16[128,128]{1,0:T(8,128)(2,1)} %tok_ref.1, f32[4,1,128]{2,1,0:T(1,128)} %bitcast.9, bf16[24,512]{1,0:T(8,128)(2,1)} %bitcast.6, bf16[24,512]{1,0:T(8,128)(2,1)} %bitcast.7, f32[1,6]{1,0:T(1,128)} %bitcast.10, ...), custom_call_target="tpu_custom_call" | custom-call | tf_op jit(solution)/shard_map/layer/pallas_call | solution.py:426
  65.6 0.0 copy-start
  65.6 8.1 %state.1 = f32[16,6,128,128]{3,2,1,0:T(8,128)} custom-call(f32[16,6,128,128]{3,2,1,0:T(8,128)} %state_ref.1, f32[6,16,128]{2,1,0:T(8,128)} %get-tuple-element.7.key_ref, f32[6,16,128]{2,1,0:T(8,128)} %get-tuple-element.8.change_ref, f32[6,16,128]{2,1,0:T(8,128)} %get-tuple-element.9.decay_ref), custom_call_target="tpu_custom_call" | custom-call | tf_op jit(solution)/shard_map/state/pallas_call | solution.py:511
  73.7 0.0 copy-done
  73.8 0.6 copy.18
Async XLA Ops:
  65.6 8.2 %copy-start = (bf16[128,128]{1,0:T(8,128)(2,1)S(1)}, bf16[128,128]{1,0:T(8,128)(2,1)}, u32[]{:S(2)}) copy-start(bf16[128,128]{1,0:T(8,128)(2,1)} %get-tuple-element.12) | copy-start | bytes 98308

commit v3 on v2

--- a/solution.py
+++ b/solution.py
@@ -10,7 +10,8 @@
 
 EPSILON = 1e-06
 CORES = 2
-VMEM_BYTES = 60 * 2**20
+VMEM_BYTES = 67043328
+SPARE_BYTES = 2**19
 BF16 = jnp.bfloat16
 F32 = jnp.float32
 
@@ -39,6 +40,11 @@
     return lax.rem(index + (offset % size), size) if offset % size else index
 
 
+def padded_bytes(shape, dtype):
+    rows, lanes = -(-shape[-2] // 16) * 16, -(-shape[-1] // 128) * 128
+    return math.prod(shape[:-2]) * rows * lanes * jnp.dtype(dtype).itemsize
+
+
 def send(src, dst, send_sem, recv_sem, device):
     copy = pltpu.make_async_remote_copy(
         src_ref=src,
@@ -60,11 +66,11 @@
     grid, all_heads, lane_gap, features,
     tok_ref, mix_ref, wb_ref, wd_ref, rate_ref, out_gain_ref, gain_ref,
     wk_hbm, wq_hbm, wv_hbm, wg_hbm, state_hbm, wout_hbm, wup_hbm, wdown_hbm,
-    out_ref, key_ref, change_ref, decay_ref,
+    out_ref, new_ref,
     cols, w_mix, w_rates, part, rate_part, rate_recv,
     near_send, near_recv, far_total, far_send, far_recv,
-    state, query_buf, value_buf, gate_buf, recalled, echoed,
-    wout, wup, wdown, mg, rs_own, rs_send, rs_recv, gathered, acc,
+    state, key_ref, change_ref, decay_ref, query_buf, value_buf, gate_buf, recalled, echoed,
+    wout, wup, wdown, mg, rs_own, rs_send, rs_recv, gathered, acc, squares_ref,
     y_own, y_send, y_recv, p_send, p_recv, last_total, f_send, f_recv,
     mix_load_sems, load_sems, own_sem, tok_sems, rate_sems, near_sems, far_sems,
     mg_sems, rs_sems, ghi_sems, gpl_sems, gco_sems, y_sems, p_sems, f_sems,
@@ -235,6 +241,16 @@
         send(own_merged, own_merged, mg_sems.at[0, k], mg_sems.at[1, k], kv_peers[k - 1])
         for k in range(1, n_kv)
     ]
+
+    @pl.loop(0, heads)
+    def _(h):
+        tall = key_ref[h].T
+        for r in range(rows):
+            row = slice(r, r + 1)
+            new_ref[r, h] = (
+                state[r, h] * decay_ref[h, row, :] + tall[:, row] * change_ref[h, row, :]
+            )
+
     loads[0].wait()
     for k in range(1, n_kv):
         started[k - 1].wait_send()
@@ -277,7 +293,7 @@
         slot = (dz * n_lo + dy) * n_x + dx
         send(place, place, gco_sems.at[0, slot], gco_sems.at[1, slot], sibling)
         other = gathered.at[index(dz, dy, dx, 1 - g.core)]
-        pending.append((place, other, gco_sems.at[0, slot], gco_sems.at[1, slot]))
+        pending.append((place, other, index(dz, dy, dx, 1 - g.core), gco_sems.at[0, slot], gco_sems.at[1, slot]))
 
     def wait_for(src, dst, send_sem, recv_sem, device):
         copy = pltpu.make_async_remote_copy(
@@ -291,6 +307,29 @@
     for dz in range(1, n_hi):
         peer = g.at(step(g.hi, dz, n_hi), g.lo, g.x, g.core)
         sent.append(send(own, own, ghi_sems.at[0, dz], ghi_sems.at[1, dz], peer))
+    loads[1].wait()
+    acc[...] = jnp.zeros_like(acc)
+    squares_ref[...] = jnp.zeros_like(squares_ref)
+
+    def absorb(chunk):
+        block = gathered[chunk].astype(F32)
+        squares_ref[...] += jnp.sum(block * block, axis=1, keepdims=True)
+        scaled = (block * gain_ref[chunk]).astype(BF16)
+        acc[...] += jnp.dot(
+            scaled, wup[pl.ds(pl.multiple_of(chunk * size, size), size), :],
+            preferred_element_type=F32,
+        )
+
+    def take_sibling(item):
+        place, other, chunk, send_sem, recv_sem = item
+        copy = pltpu.make_async_remote_copy(
+            src_ref=place, dst_ref=other, send_sem=send_sem, recv_sem=recv_sem,
+            device_id=sibling, device_id_type=pl.DeviceIdType.MESH,
+        )
+        copy.wait_recv()
+        copy.wait_send()
+        absorb(chunk)
+
     for dz in range(n_hi):
         place = gathered.at[index(dz, 0, 0, g.core)]
         if dz:
@@ -300,48 +339,24 @@
             sent.append(send(place, place, gpl_sems.at[0, dz, p], gpl_sems.at[1, dz, p],
                              plane_peers[d]))
         to_sibling(dz, 0, 0)
+        absorb(index(dz, 0, 0, g.core))
     for dz in range(n_hi):
         for p, (dy, dx) in enumerate(g.plane):
             place = gathered.at[index(dz, dy, dx, g.core)]
             wait_for(own, place, gpl_sems.at[0, dz, p], gpl_sems.at[1, dz, p],
                      plane_peers[dy, dx])
             to_sibling(dz, dy, dx)
+            absorb(index(dz, dy, dx, g.core))
+            if pending:
+                take_sibling(pending.pop(0))
+    for item in pending:
+        take_sibling(item)
     for copy in sent:
         copy.wait_send()
-    for place, other, send_sem, recv_sem in pending:
-        copy = pltpu.make_async_remote_copy(
-            src_ref=place, dst_ref=other, send_sem=send_sem, recv_sem=recv_sem,
-            device_id=sibling, device_id_type=pl.DeviceIdType.MESH,
-        )
-        copy.wait_recv()
-        copy.wait_send()
 
     n_dev = n_kv * n_tp
-
-    def add_squares(i, total):
-        block = gathered[i].astype(F32)
-        return total + jnp.sum(block * block, axis=1, keepdims=True)
-
-    squares = lax.fori_loop(0, n_dev, add_squares, jnp.zeros((batch, 1), F32))
-    scale = lax.rsqrt(squares / features + EPSILON)
-    group = n_tp if size % 128 == 0 else 1
-    loads[1].wait()
-    acc[...] = jnp.zeros_like(acc)
-
-    @pl.loop(0, n_dev // group)
-    def _(i):
-        parts = [
-            (gathered[i * group + j].astype(F32) * scale * gain_ref[i * group + j]).astype(BF16)
-            for j in range(group)
-        ]
-        block = parts[0] if group == 1 else jnp.concatenate(parts, axis=1)
-        depth = group * size
-        acc[...] += jnp.dot(
-            block, wup[pl.ds(pl.multiple_of(i * depth, depth), depth), :],
-            preferred_element_type=F32,
-        )
-
-    hidden = jnp.square(jnp.maximum(acc[...], 0.0)).astype(BF16)
+    scale = lax.rsqrt(squares_ref[...] / (n_dev * size) + EPSILON)
+    hidden = jnp.square(jnp.maximum(acc[...] * scale, 0.0)).astype(BF16)
     loads[2].wait()
     width = n_tp * size
 
@@ -419,55 +434,60 @@
     lanes = -(-(2 * lane_gap + 1) // 128) * 128
     n_plane = max(1, len(g.plane))
     vmem = pl.BlockSpec(memory_space=pltpu.VMEM)
-    hbm = pl.BlockSpec(memory_space=pl.ANY)
+    hbm = pl.BlockSpec(memory_space=pltpu.HBM)
     dma = pltpu.SemaphoreType.DMA
     block = (batch, size)
     per_head = (heads, rows, head_size)
+    buffers = [
+        pltpu.VMEM((g.n_tp,) + block, BF16),
+        pltpu.VMEM((4, depth, width), BF16),
+        pltpu.VMEM((lanes, depth), BF16),
+        pltpu.VMEM((4, g.n_kv, rows, width), F32),
+        pltpu.VMEM((g.n_kv, rows, lanes), F32),
+        pltpu.VMEM((g.n_kv, rows, lanes), F32),
+        pltpu.VMEM((4, g.n_lo, g.n_hi, rows, width), BF16),
+        pltpu.VMEM((4, g.n_lo, g.n_hi, rows, width), BF16),
+        pltpu.VMEM((4, rows, width), F32),
+        pltpu.VMEM((4, g.n_hi, rows, width), BF16),
+        pltpu.VMEM((4, g.n_hi, rows, width), BF16),
+        pltpu.VMEM(state.shape, F32),
+        pltpu.VMEM(per_head, F32),
+        pltpu.VMEM(per_head, F32),
+        pltpu.VMEM(per_head, F32),
+        pltpu.VMEM(per_head, F32),
+        pltpu.VMEM((rows, width), F32),
+        pltpu.VMEM((rows, width), F32),
+        pltpu.VMEM(per_head, F32),
+        pltpu.VMEM(per_head, F32),
+        pltpu.VMEM(w_out.shape, BF16),
+        pltpu.VMEM(w_up.shape, BF16),
+        pltpu.VMEM(w_down.shape, BF16),
+        pltpu.VMEM((g.n_kv, rows, width), BF16),
+        pltpu.VMEM((g.n_tp,) + block, F32),
+        pltpu.VMEM((g.n_tp,) + block, BF16),
+        pltpu.VMEM((g.n_tp,) + block, BF16),
+        pltpu.VMEM((n_dev,) + block, BF16),
+        pltpu.VMEM((batch, w_up.shape[1]), F32),
+        pltpu.VMEM((batch, 1), F32),
+        pltpu.VMEM((g.n_kv, g.n_x) + block, F32),
+        pltpu.VMEM((g.n_kv, g.n_x) + block, BF16),
+        pltpu.VMEM((g.n_kv, g.n_x) + block, BF16),
+        pltpu.VMEM((g.n_hi, n_plane) + block, BF16),
+        pltpu.VMEM((g.n_hi, n_plane) + block, BF16),
+        pltpu.VMEM((g.n_hi,) + block, F32),
+        pltpu.VMEM((g.n_hi,) + block, BF16),
+        pltpu.VMEM((g.n_hi,) + block, BF16),
+    ]
+    limit = VMEM_BYTES - SPARE_BYTES - padded_bytes(state.shape, F32)
     return pl.pallas_call(
         functools.partial(layer_kernel, g, all_heads, lane_gap, n_dev * size),
         out_shape=(
             jax.ShapeDtypeStruct(block, BF16),
-            jax.ShapeDtypeStruct(per_head, F32),
-            jax.ShapeDtypeStruct(per_head, F32),
-            jax.ShapeDtypeStruct(per_head, F32),
+            pltpu.VMEM(state.shape, F32),
         ),
         in_specs=[vmem] * 7 + [hbm] * 8,
-        out_specs=(vmem,) * 4,
-        scratch_shapes=[
-            pltpu.VMEM((g.n_tp,) + block, BF16),
-            pltpu.VMEM((4, depth, width), BF16),
-            pltpu.VMEM((lanes, depth), BF16),
-            pltpu.VMEM((4, g.n_kv, rows, width), F32),
-            pltpu.VMEM((g.n_kv, rows, lanes), F32),
-            pltpu.VMEM((g.n_kv, rows, lanes), F32),
-            pltpu.VMEM((4, g.n_lo, g.n_hi, rows, width), BF16),
-            pltpu.VMEM((4, g.n_lo, g.n_hi, rows, width), BF16),
-            pltpu.VMEM((4, rows, width), F32),
-            pltpu.VMEM((4, g.n_hi, rows, width), BF16),
-            pltpu.VMEM((4, g.n_hi, rows, width), BF16),
-            pltpu.VMEM(state.shape, F32),
-            pltpu.VMEM(per_head, F32),
-            pltpu.VMEM((rows, width), F32),
-            pltpu.VMEM((rows, width), F32),
-            pltpu.VMEM(per_head, F32),
-            pltpu.VMEM(per_head, F32),
-            pltpu.VMEM(w_out.shape, BF16),
-            pltpu.VMEM(w_up.shape, BF16),
-            pltpu.VMEM(w_down.shape, BF16),
-            pltpu.VMEM((g.n_kv, rows, width), BF16),
-            pltpu.VMEM((g.n_tp,) + block, F32),
-            pltpu.VMEM((g.n_tp,) + block, BF16),
-            pltpu.VMEM((g.n_tp,) + block, BF16),
-            pltpu.VMEM((n_dev,) + block, BF16),
-            pltpu.VMEM((batch, w_up.shape[1]), F32),
-            pltpu.VMEM((g.n_kv, g.n_x) + block, F32),
-            pltpu.VMEM((g.n_kv, g.n_x) + block, BF16),
-            pltpu.VMEM((g.n_kv, g.n_x) + block, BF16),
-            pltpu.VMEM((g.n_hi, n_plane) + block, BF16),
-            pltpu.VMEM((g.n_hi, n_plane) + block, BF16),
-            pltpu.VMEM((g.n_hi,) + block, F32),
-            pltpu.VMEM((g.n_hi,) + block, BF16),
-            pltpu.VMEM((g.n_hi,) + block, BF16),
+        out_specs=(vmem,) * 2,
+        scratch_shapes=buffers + [
             dma((4,)),
             dma((4,)),
             dma,
@@ -485,7 +505,7 @@
             dma((2, g.n_hi)),
         ],
         compiler_params=pltpu.CompilerParams(
-            collective_id=0, has_side_effects=True, vmem_limit_bytes=VMEM_BYTES
+            collective_id=0, has_side_effects=True, vmem_limit_bytes=limit
         ),
         name="layer",
     )(
@@ -495,40 +515,15 @@
     )
 
 
-def state_kernel(state_ref, key_ref, change_ref, decay_ref, new_ref):
-    tall = key_ref[0].T
-    for r in range(state_ref.shape[0]):
-        row = slice(r, r + 1)
-        new_ref[r, 0] = (
-            state_ref[r, 0] * decay_ref[0, row, :] + tall[:, row] * change_ref[0, row, :]
-        )
-
-
-def write_state(state, key, change, decay):
-    rows, heads, size, _ = state.shape
-    whole = pl.BlockSpec((rows, 1, size, size), lambda i: (0, i, 0, 0))
-    small = pl.BlockSpec((1, rows, size), lambda i: (i, 0, 0))
-    return pl.pallas_call(
-        state_kernel,
-        grid=(heads,),
-        out_shape=jax.ShapeDtypeStruct(state.shape, F32),
-        in_specs=[whole, small, small, small],
-        out_specs=whole,
-        compiler_params=pltpu.CompilerParams(dimension_semantics=("arbitrary",)),
-        name="state",
-    )(state, key, change, decay)
-
-
 def local(
     n_kv, n_tp,
     tokens, mix_gain, w_query, w_key, w_value, w_gate, w_beta, w_decay, decay_rate, out_gain,
     state, w_out, mlp_gain, w_up, w_down,
 ):
-    mixed, key, change, decay = layer(
+    return layer(
         Grid(n_kv, n_tp), tokens, mix_gain, (w_key, w_query, w_value, w_gate), w_beta, w_decay,
         decay_rate, out_gain, state, w_out, mlp_gain, w_up, w_down,
     )
-    return (mixed, write_state(state, key, change, decay))
 
 
 def solution(mesh):

time: 74.7 us -> 65.7 us (0.88)
  Pallas kernels: 73.1 us -> 61.5 us
  local copies, waits for them, and re-layouts: 0.62 us -> 3.32 us
    pallas_call x1 -> x0, Pallas kernels: 8.14 us -> none  [write_state(): pl.pallas_call(state_kernel, grid=(heads,), out_shape=jax.ShapeDtypeStruc...]
    pallas_call x1, Pallas kernels: 65 us -> 61.5 us  [layer(): pl.pallas_call(functools.partial(layer_kernel, g, all_heads, lane_gap, n_...]
    unnamed x3 -> x4, local copies, waits for them, and re-layouts: 0.62 us -> 3.32 us
where the time goes in v3:
time: 65.7 us; the launch traced here: 65.4 us
  Pallas kernels  61.5 us (94%)
  local copies, waits for them, and re-layouts  3.32 us (5%)
    pallas_call x1, Pallas kernels, layer(): pl.pallas_call(functools.partial(layer_kernel, g, all_heads, lane_gap, n_...  61.5 us
    unnamed x4, local copies, waits for them, and re-layouts  3.32 us

profile of v3, /device:TPU:0, one launch (start us, length us, event | category | flops | bytes accessed | tf_op | source)
XLA Modules:
  0.0 65.4 jit_solution(5925984071726284326)
XLA Ops:
  0.6 61.5 %layer.1 = (bf16[128,128]{1,0:T(8,128)(2,1)}, f32[16,6,128,128]{3,2,1,0:T(8,128)S(1)}) custom-call(bf16[128,128]{1,0:T(8,128)(2,1)} %tok_ref.1, f32[4,1,128]{2,1,0:T(1,128)} %bitcast.9, bf16[24,512]{1,0:T(8,128)(2,1)} %bitcast.6, bf16[24,512]{1,0:T(8,128)(2,1)} %bitcast.7, f32[1,6]{1,0:T(1,128)} %bitcast.10, f32[1,128]{1,0:T(1,128)} %bitcast.11, ...), custom_call_target="tpu_custom_call" | custom-call | tf_op jit(solution)/shard_map/layer/pallas_call | solution.py:482
  62.1 0.0 copy-start
  62.1 2.7 %copy.19 = f32[16,6,128,128]{3,2,1,0:T(8,128)} copy(f32[16,6,128,128]{3,2,1,0:T(8,128)S(1)} %get-tuple-element.3) | data formatting | bytes 12582912
  64.8 0.0 copy-done
  64.8 0.6 copy.20
Async XLA Ops:
  62.1 2.7 %copy-start = (bf16[128,128]{1,0:T(8,128)(2,1)S(1)}, bf16[128,128]{1,0:T(8,128)(2,1)}, u32[]{:S(2)}) copy-start(bf16[128,128]{1,0:T(8,128)(2,1)} %get-tuple-element.6) | copy-start | bytes 98308
